TPU v7x, 512 devices: a whole 4x8x8 slice. The times are simulated.
512 devices in a mesh: sp: 32 (over z, x), dp: 16 (over y, core).
Axes of the slice: x: 4, y: 8, z: 8, core: 2. Of those that a mesh axis runs over, the one named last changes fastest.
Arguments:
- query_rows: bfloat16 [16, 4096, 2048], P('dp', 'sp'), may hold values from -6 to 6
- key_rows: bfloat16 [16, 4096, 2048], P('dp', 'sp'), may hold values from -6 to 6
- value_rows: bfloat16 [16, 4096, 2048], P('dp', 'sp'), may hold values from -6 to 6
- decay_low: bfloat16 [16, 4096, 128], P('dp', 'sp'), may hold values from -5 to 5
- rate_low: bfloat16 [16, 4096, 128], P('dp', 'sp'), may hold values from -4 to 4
- decay_up: bfloat16 [128, 2048], replicated, may hold values from -0.5 to 0.5
- rate_up: bfloat16 [128, 2048], replicated, may hold values from -0.5 to 0.5
- decay_base: float32 [2048], replicated, may hold values from -12 to -2
- norm_gain: float32 [2048], replicated, may hold values from 0.1 to 1.9
- out_weight: bfloat16 [2048, 2048], P(None, 'dp'), may hold values from -0.125 to 0.125
Outputs:
- layer_out: bfloat16 [16, 4096, 2048], P('dp', 'sp')
All inputs are finite; a program needn't handle non-finite values.
Results may differ from a plain program's by a relative error of at most 0.005.
Values may be sent and summed in bfloat16 or wider, within the bound.
A program may use at most 128 MiB of HBM per device.

v0:
```python
import functools
import math

import jax
import jax.numpy as jnp
from jax import lax
from jax.experimental import pallas as pl
from jax.experimental.pallas import tpu as pltpu
from jax.sharding import PartitionSpec as P

HEAD = 64
PAIR = 2 * HEAD

F32 = jnp.float32
BF16 = jnp.bfloat16


def mm(left, right):
    return lax.dot_general(left, right, (((1,), (0,)), ((), ())), preferred_element_type=F32)


def mm_nt(left, right):
    return lax.dot_general(left, right, (((1,), (1,)), ((), ())), preferred_element_type=F32)


def mm_tn(left, right):
    return lax.dot_general(left, right, (((0,), (0,)), ((), ())), preferred_element_type=F32)


def split(x):
    high = x.astype(BF16)
    return high, (x - high.astype(F32)).astype(BF16)


def mm3(left, right, form=mm):
    return form(left[0], right[0]) + form(left[0], right[1]) + form(left[1], right[0])


def iota(shape, dim):
    return lax.broadcasted_iota(jnp.int32, shape, dim)


def first_half(shape):
    return iota(shape, len(shape) - 1) < HEAD


def stack_pair(x):
    here = lax.rem(iota(x.shape, 1), PAIR) < HEAD
    zero = jnp.zeros_like(x)
    return jnp.concatenate([jnp.where(here, x, zero), jnp.where(here, zero, x)], axis=0)


def head_ones(scale):
    row = iota((2 * PAIR, PAIR), 0)
    col = iota((2 * PAIR, PAIR), 1)
    same = (lax.rem(row, PAIR) // HEAD) == (col // HEAD)
    return jnp.where(same, F32(scale), F32(0.0)).astype(BF16)


def head_sum(x, ones):
    return mm(jnp.concatenate(split(x), axis=1), ones)


def inverse_levels(strict_parts, size):
    row = iota((size, size), 0)
    col = iota((size, size), 1)
    eye = jnp.where(row == col, F32(1.0), F32(0.0))
    found = None
    block = 1
    while block < size:
        pick = (row // (2 * block) == col // (2 * block)) & (row // block != col // block) & (row > col)
        pieces = [jnp.where(pick, high, jnp.zeros_like(high)) for high, _ in strict_parts]
        if found is None:
            found = [eye.astype(BF16) - p for p in pieces]
        else:
            right = [mm(p, x).astype(BF16) for p, x in zip(pieces, found)]
            found = [x - mm(x, y).astype(BF16) for x, y in zip(found, right)]
        block *= 2
    out = []
    for (high, low), x in zip(strict_parts, found):
        product = mm(jnp.concatenate([high, low], axis=1), jnp.concatenate([x, x], axis=0))
        residual = ((eye - x.astype(F32)) - product).astype(BF16)
        out.append((x, mm(x, residual).astype(BF16)))
    return out


def gates(squashed, rate_low, decay_up, rate_up, base):
    decay_pre = (base + mm(squashed, decay_up)).astype(BF16).astype(F32)
    rate_pre = mm(rate_low, rate_up).astype(BF16).astype(F32)
    log_decay = -math.exp(-0.5) / (1.0 + jnp.exp(-decay_pre))
    rate = 1.0 / (1.0 + jnp.exp(-rate_pre))
    return log_decay, rate


def local_pairs(pairs):
    size = pairs[0][0].shape[0]
    middle = size // 2
    row = iota((size, size), 0)
    col = iota((size, size), 1)
    strict = row > col
    within = row >= col
    upto = jnp.where(within, F32(1.0), F32(0.0)).astype(BF16)
    upto = jnp.concatenate([upto, upto], axis=1)
    ones = head_ones(1.0)
    made = []
    strict_parts = []
    for q, k, v, log_decay, rate in pairs:
        q = q.astype(F32)
        k = k.astype(F32)
        running = mm(upto, jnp.concatenate(split(log_decay), axis=0))
        centre = running[middle : middle + 1]
        final = running[size - 1 :]
        ahead = jnp.exp(running - centre)
        ahead_before = jnp.exp(running - log_decay - centre)
        behind = jnp.exp(centre - running)
        unit = k * lax.rsqrt(1.0 + head_sum(k * k, ones))
        erase = unit * rate
        at_centre = jnp.exp(centre)
        at_end = jnp.exp(final - centre)
        read_mid = q * ahead
        erase_from = unit * ahead_before
        key_to = k * behind
        erase_to = erase * behind
        left = split(jnp.concatenate([stack_pair(erase_from), stack_pair(read_mid)], axis=0))
        right = split(jnp.concatenate([key_to, erase_to], axis=0))
        grid = mm_nt(
            jnp.concatenate(left, axis=1), jnp.concatenate([right[0], right[0]], axis=1)
        ) + mm_nt(left[0], right[1])
        part = lambda i, j, keep: jnp.where(
            keep, grid[i * size : (i + 1) * size, j * size : (j + 1) * size], 0.0
        )
        key_pairs = split(jnp.concatenate([part(0, 0, strict), part(1, 0, strict)], axis=1))
        strict_parts += [split(part(0, 1, strict)), split(part(1, 1, strict))]
        read_keys = split(jnp.concatenate([part(2, 0, within), part(3, 0, within)], axis=1))
        read_erase = split(jnp.concatenate([part(2, 1, within), part(3, 1, within)], axis=1))
        values = stack_pair(v)
        carried = mm(key_pairs[0], values) + mm(key_pairs[1], values)
        kept = mm(read_keys[0], values) + mm(read_keys[1], values)
        sides = jnp.concatenate([erase_from * at_centre, carried], axis=1)
        made.append((
            v, sides, kept, read_erase, read_mid * at_centre,
            key_to * at_end, erase_to * at_end, jnp.exp(final),
        ))
    inverses = inverse_levels(strict_parts, size)
    out = []
    for i, (v, sides, kept, read_erase, read_start, key_end, erase_end, decay_all) in enumerate(made):
        xa, xb = inverses[2 * i], inverses[2 * i + 1]
        inv = tuple(jnp.concatenate([a, b], axis=1) for a, b in zip(xa, xb))
        solved = mm3(inv, split(stack_pair(sides)))
        parts = split(solved)
        taken = mm3(read_erase, tuple(stack_pair(p) for p in parts))
        read_state = read_start - taken[:, :PAIR]
        readout = kept - taken[:, PAIR:]
        key_parts = split(key_end)
        erase_parts = split(erase_end)
        moved = mm3(erase_parts, parts, mm_tn)
        gained = mm_tn(key_parts[0], v) + mm_tn(key_parts[1], v)
        row2 = iota((PAIR, PAIR), 0)
        col2 = iota((PAIR, PAIR), 1)
        transfer = jnp.where(row2 == col2, jnp.broadcast_to(decay_all, (PAIR, PAIR)), 0.0) - moved[:, :PAIR]
        added = gained - moved[:, PAIR:]
        half = first_half((HEAD, PAIR))
        fold = lambda x: jnp.where(half, x[:HEAD], x[HEAD:])
        out.append((fold(transfer), fold(added), read_state, readout))
    return out


def local_kernel(count, q_ref, k_ref, v_ref, low_ref, rate_ref, dup_ref, rup_ref, base_ref,
                 transfer_ref, added_ref, state_ref, readout_ref):
    squashed = jnp.tanh(low_ref[...].astype(F32)).astype(BF16)
    log_decay, rate = gates(squashed, rate_ref[...], dup_ref[...], rup_ref[...], base_ref[...])
    pairs = []
    for i in range(count):
        at = slice(i * PAIR, (i + 1) * PAIR)
        pairs.append((q_ref[:, at], k_ref[:, at], v_ref[:, at], log_decay[:, at], rate[:, at]))
    for i, (transfer, added, state, readout) in enumerate(local_pairs(pairs)):
        at = slice(i * PAIR, (i + 1) * PAIR)
        transfer_ref[:, at] = transfer
        added_ref[:, at] = added
        state_ref[:, at] = state
        readout_ref[:, at] = readout


def local_block(q, k, v, decay_low, rate_low, decay_up, rate_up, base):
    size, width = q.shape
    low = decay_low.shape[1]
    count = math.gcd(width // PAIR, 2)
    lanes = count * PAIR
    cols = lambda rows: pl.BlockSpec((rows, lanes), lambda i: (0, i))
    whole = pl.BlockSpec((size, low), lambda i: (0, 0))
    return pl.pallas_call(
        functools.partial(local_kernel, count),
        grid=(width // lanes,),
        in_specs=[cols(size)] * 3 + [whole] * 2 + [cols(low)] * 2 + [cols(1)],
        out_specs=[cols(HEAD), cols(HEAD), cols(size), cols(size)],
        out_shape=[
            jax.ShapeDtypeStruct((HEAD, width), F32),
            jax.ShapeDtypeStruct((HEAD, width), F32),
            jax.ShapeDtypeStruct((size, width), F32),
            jax.ShapeDtypeStruct((size, width), F32),
        ],
        cost_estimate=pl.CostEstimate(flops=10**10, bytes_accessed=10**7, transcendentals=0),
        name="local_block",
    )(q, k, v, decay_low, rate_low, decay_up, rate_up, base)


def chain_kernel(devices, group, transfer_ref, added_ref, state_ref, readout_ref, gain_ref,
                 mix_ref, start_buf, end_buf, send_sem, recv_sem):
    me = lax.axis_index("sp")
    groups = transfer_ref.shape[1] // group
    has_left = me > 0
    has_right = me < devices - 1
    barrier = pltpu.get_barrier_semaphore()

    @pl.when(has_left)
    def _():
        pl.semaphore_signal(barrier, inc=1, device_id={"sp": me - 1}, device_id_type=pl.DeviceIdType.MESH)

    @pl.when(has_right)
    def _():
        pl.semaphore_signal(barrier, inc=1, device_id={"sp": me + 1}, device_id_type=pl.DeviceIdType.MESH)

    pl.semaphore_wait(barrier, jnp.minimum(me, 1) + jnp.minimum(devices - 1 - me, 1))

    def copy(g):
        return pltpu.make_async_remote_copy(
            src_ref=end_buf.at[g],
            dst_ref=start_buf.at[g],
            send_sem=send_sem.at[g],
            recv_sem=recv_sem.at[g],
            device_id={"sp": lax.rem(me + 1, devices)},
            device_id_type=pl.DeviceIdType.MESH,
        )

    mean_ones = head_ones(1.0 / HEAD)

    @pl.when(jnp.logical_not(has_left))
    def _():
        start_buf[...] = jnp.zeros_like(start_buf)

    for g in range(groups):
        @pl.when(has_left)
        def _():
            copy(g).wait_recv()

        starts = []
        for i in range(group // PAIR):
            at = slice(g * group + i * PAIR, g * group + (i + 1) * PAIR)
            here = slice(i * PAIR, (i + 1) * PAIR)
            start = split(stack_pair(start_buf[g, :, here]))
            end_buf[g, :, here] = mm3(split(transfer_ref[:, at]), start) + added_ref[:, at]
            starts.append(start)

        @pl.when(has_right)
        def _():
            copy(g).start()

        for i, start in enumerate(starts):
            at = slice(g * group + i * PAIR, g * group + (i + 1) * PAIR)
            readout = mm3(split(state_ref[:, at]), start) + readout_ref[:, at]
            centred = readout - head_sum(readout, mean_ones)
            variance = head_sum(centred * centred, mean_ones)
            mix_ref[:, at] = (centred * lax.rsqrt(variance + 1.0) * gain_ref[:, at]).astype(BF16)

    @pl.when(has_right)
    def _():
        for g in range(groups):
            copy(g).wait_send()


def chain(devices, transfer, added, state, readout, gain):
    size, width = state.shape
    group = PAIR * math.gcd(width // PAIR, 2)
    groups = width // group
    vmem = pl.BlockSpec(memory_space=pltpu.VMEM)
    return pl.pallas_call(
        functools.partial(chain_kernel, devices, group),
        in_specs=[vmem] * 5,
        out_specs=vmem,
        out_shape=jax.ShapeDtypeStruct((size, width), BF16),
        scratch_shapes=[
            pltpu.VMEM((groups, HEAD, group), F32),
            pltpu.VMEM((groups, HEAD, group), F32),
            pltpu.SemaphoreType.DMA((groups,)),
            pltpu.SemaphoreType.DMA((groups,)),
        ],
        compiler_params=pltpu.CompilerParams(collective_id=0, has_side_effects=True),
        cost_estimate=pl.CostEstimate(flops=10**10, bytes_accessed=10**7, transcendentals=0),
        name="state_chain",
    )(transfer, added, state, readout, gain)


def per_device(devices, query_rows, key_rows, value_rows, decay_low, rate_low, decay_up, rate_up,
               decay_base, norm_gain, out_weight):
    weight = lax.all_gather(out_weight, "dp", axis=1, tiled=True)
    made = local_block(
        query_rows[0], key_rows[0], value_rows[0], decay_low[0], rate_low[0],
        decay_up, rate_up, decay_base[None],
    )
    mix = chain(devices, *made, norm_gain[None])
    return jnp.dot(mix, weight, preferred_element_type=F32).astype(BF16)[None]


def solution(mesh):
    in_specs = (
        P("dp", "sp", None),
        P("dp", "sp", None),
        P("dp", "sp", None),
        P("dp", "sp", None),
        P("dp", "sp", None),
        P(),
        P(),
        P(),
        P(),
        P(None, "dp"),
    )
    return jax.shard_map(
        functools.partial(per_device, mesh.shape["sp"]),
        mesh=mesh, in_specs=in_specs, out_specs=P("dp", "sp", None), check_vma=False,
    )
```

profile of v0, /device:TPU:502, one launch (start us, length us, event | category | flops | bytes accessed | tf_op | source)
XLA Modules:
  0.0 183.2 jit_solution(13905479529959106889)
XLA Ops:
  6.5 0.0 all-gather.2.cloned.1.call-start
  6.5 0.7 all-gather.2.cloned.1.call-update
  7.3 38.7 %local_block.1 = (f32[64,2048]{1,0:T(8,128)}, f32[64,2048]{1,0:T(8,128)}, f32[128,2048]{1,0:T(8,128)}, f32[128,2048]{1,0:T(8,128)}) custom-call(bf16[128,2048]{1,0:T(8,128)(2,1)} %bitcast.11, bf16[128,2048]{1,0:T(8,128)(2,1)} %bitcast.12, bf16[128,2048]{1,0:T(8,128)(2,1)} %bitcast.13, bf16[128,128]{1,0:T(8,128)(2,1)} %bitcast.14, bf16[128,128]{1,0:T(8,128)(2,1)} %bitcast.15, ...), custom_call_target="tpu_custom_call" | custom-call | flops 10000000000 | bytes 10000000 | tf_op jit(solution)/shard_map/local_block/pallas_call | solution.py:191
  45.9 124.8 %state_chain.1 = bf16[128,2048]{1,0:T(8,128)(2,1)} custom-call(f32[64,2048]{1,0:T(8,128)} %get-tuple-element.9.transfer_ref, f32[64,2048]{1,0:T(8,128)} %get-tuple-element.10.added_ref, f32[128,2048]{1,0:T(8,128)} %get-tuple-element.11.state_ref, f32[128,2048]{1,0:T(8,128)} %get-tuple-element.12.readout_ref, f32[1,2048]{1,0:T(1,128)} %bitcast.17), custom_call_target="tpu_custom_call" | custom-call | flops 10000000000 | bytes 10000000 | tf_op jit(solution)/shard_map/state_chain/pallas_call | solution.py:276
  170.8 0.0 all-gather.2.cloned.1.call-done
  170.8 5.6 %fusion = bf16[1,128,2048]{2,1,0:T(8,128)(2,1)} fusion(bf16[128,2048]{1,0:T(8,128)(2,1)} %state_chain.1, bf16[2048,2048]{1,0:T(8,128)(2,1)} %all-gather.2.cloned.1.call-done), kind=kOutput, calls=%fused_computation.1 | convolution fusion | flops 1074003968 | bytes 9437184 | tf_op jit(solution)/shard_map/dot_general | solution.py:301
Async XLA Ops:
  6.5 164.2 %all-gather.2.cloned.1.call-start = ((), (), s32[]{:S(2)}) async-start(), calls=%async_computation | async-start | bytes 8912896 | tf_op jit(solution)/shard_map/all_gather | solution.py:295
Sparse Core Ops, SparseCore 0:
  9.4 64.0 all-gather.1
where the time goes:
time: 183 us
  Pallas kernels  163 us (89%)
  between operations  13.4 us (7%)
  matrix products  5.62 us (3%)
    pallas_call x1, Pallas kernels, chain(): pl.pallas_call(functools.partial(chain_kernel, devices, group), in_specs=...  125 us
    pallas_call x1, Pallas kernels, local_block(): pl.pallas_call(functools.partial(local_kernel, count), grid=(width // lan...  38.7 us
    dot_general x1, matrix products, per_device(): return jnp.dot(mix, weight, preferred_element_type=F32).astype(BF16)[None]  5.62 us
  transfers between devices with their start and end apart: 1, of which 0 were waited for; matrix products, arithmetic and copies ran while one was open for 0% of the time, Pallas kernels for 89%

commit v1 on v0

v1 whole, which is shorter than its diff:
```python
import functools
import math

import jax
import jax.numpy as jnp
from jax import lax
from jax.experimental import pallas as pl
from jax.experimental.pallas import tpu as pltpu
from jax.sharding import PartitionSpec as P

HEAD = 64
PAIR = 2 * HEAD
QUAD = 2 * PAIR
XDIM = 4

F32 = jnp.float32
BF16 = jnp.bfloat16
MESH = pl.DeviceIdType.MESH


def mm(left, right):
    return lax.dot_general(left, right, (((1,), (0,)), ((), ())), preferred_element_type=F32)


def mm_nt(left, right):
    return lax.dot_general(left, right, (((1,), (1,)), ((), ())), preferred_element_type=F32)


def mm_tn(left, right):
    return lax.dot_general(left, right, (((0,), (0,)), ((), ())), preferred_element_type=F32)


def split(x):
    high = x.astype(BF16)
    return high, (x - high.astype(F32)).astype(BF16)


def iota(shape, dim):
    return lax.broadcasted_iota(jnp.int32, shape, dim)


def cat(parts, axis):
    return jnp.concatenate(parts, axis=axis)


def diag2(a, b):
    return cat([cat([a, jnp.zeros_like(b)], 1), cat([jnp.zeros_like(a), b], 1)], 0)


def swap_halves(x):
    return pltpu.roll(x.astype(F32), HEAD, 1).astype(x.dtype)


def low_half(shape):
    return lax.rem(iota(shape, 1), PAIR) < HEAD


def stack_pair(x):
    here = low_half(x.shape)
    zero = jnp.zeros_like(x)
    return cat([jnp.where(here, x, zero), jnp.where(here, zero, x)], 0)


def same_head_ones(width, scale):
    same = (iota((width, width), 0) // HEAD) == (iota((width, width), 1) // HEAD)
    return jnp.where(same, F32(scale), F32(0.0)).astype(BF16)


def put_split(refs, at, x):
    high, low = split(x)
    refs[0][:, at] = high
    refs[1][:, at] = low


def prepare(size, at, q_ref, k_ref, squashed, rate_low, dup_ref, rup_ref, base_ref, ops, decay_buf, pair):
    middle = size // 2
    upto = jnp.where(iota((size, size), 0) >= iota((size, size), 1), F32(1.0), F32(0.0)).astype(BF16)
    upto = cat([upto, upto], 1)
    decay_pre = (base_ref[:, at] + mm(squashed, dup_ref[:, at])).astype(BF16).astype(F32)
    rate_pre = mm(rate_low, rup_ref[:, at]).astype(BF16).astype(F32)
    log_decay = -math.exp(-0.5) / (1.0 + jnp.exp(-decay_pre))
    rate = 1.0 / (1.0 + jnp.exp(-rate_pre))
    running = mm(upto, cat(split(log_decay), 0))
    centre = running[middle : middle + 1]
    final = running[size - 1 :]
    ahead = jnp.exp(running - centre)
    before = jnp.exp(running - log_decay - centre)
    behind = jnp.exp(centre - running)
    at_centre = jnp.exp(centre)
    at_end = jnp.exp(final - centre)
    k = k_ref[:, at].astype(F32)
    q = q_ref[:, at].astype(F32)
    unit = k * lax.rsqrt(1.0 + mm(cat(split(k * k), 1), cat([same_head_ones(QUAD, 1.0)] * 2, 0)))
    erase_from = unit * before
    read_mid = q * ahead
    key_to = k * behind
    erase_to = -(unit * rate) * behind
    put_split(ops["from"], at, erase_from)
    put_split(ops["read"], at, read_mid)
    put_split(ops["key"], at, key_to)
    put_split(ops["erase"], at, erase_to)
    ops["from_start"][:, at] = erase_from * at_centre
    ops["read_start"][:, at] = read_mid * at_centre
    ops["key_end"][:, at] = (key_to * at_end).astype(BF16)
    ops["erase_end"][:, at] = (erase_to * at_end).astype(BF16)
    decays = jnp.exp(final)
    for i in range(2):
        here = decays[:, i * PAIR : (i + 1) * PAIR]
        decay_buf[2 * (pair + i)] = here
        decay_buf[2 * (pair + i) + 1] = pltpu.roll(here, HEAD, 1)


def by_head(x):
    return diag2(x[:, :PAIR], x[:, PAIR:])


def grids(size, left, ops, at, keep):
    high, low = (stack_pair(ref[:, at]) for ref in left)
    right = cat([ops["key"][0][:, at], ops["erase"][0][:, at]], 0)
    rest = cat([ops["key"][1][:, at], ops["erase"][1][:, at]], 0)
    grid = mm_nt(cat([high, low], 1), cat([right, right], 1)) + mm_nt(high, rest)
    part = lambda i, j: jnp.where(keep, grid[i * size : (i + 1) * size, j * size : (j + 1) * size], 0.0)
    return split(cat([part(0, 0), part(1, 0)], 1)), split(cat([part(0, 1), part(1, 1)], 1))


def inverses(splits, size):
    negs = [high for high, _ in splits]
    row = iota((size, PAIR * 2), 0)
    col = lax.rem(iota((size, PAIR * 2), 1), PAIR)
    eye = jnp.where(row == col, F32(1.0), F32(0.0)).astype(BF16)
    found = None
    block = 1
    while block < size:
        pick = (row // (2 * block) == col // (2 * block)) & (row // block != col // block) & (row > col)
        pieces = [jnp.where(pick, n, jnp.zeros_like(n)) for n in negs]
        if found is None:
            found = [eye + p for p in pieces]
        elif block < 16:
            right = [mm(p, by_head(x)).astype(BF16) for p, x in zip(pieces, found)]
            found = [x + mm(x, by_head(y)).astype(BF16) for x, y in zip(found, right)]
        else:
            starts = list(range(block, size, 2 * block))
            take = lambda m: cat([m[s : s + block] for s in starts], 0) if len(starts) > 1 else m[block:]
            right = [mm(take(p), by_head(x)).astype(BF16) for p, x in zip(pieces, found)]
            blank = jnp.zeros((block, 2 * PAIR), BF16)
            spread = lambda m: cat(
                [part for j in range(len(starts)) for part in (blank, m[j * block : (j + 1) * block])], 0)
            right = [spread(y) for y in right]
            step = [mm(take(x), by_head(y)).astype(BF16) for x, y in zip(found, right)]
            found = [x + spread(t) for x, t in zip(found, step)]
        block *= 2
    out = []
    for (high, low), x in zip(splits, found):
        residual = (eye - x).astype(F32) + (mm(high, by_head(x)) + mm(low, by_head(x)))
        out.append((x, mm(x, by_head(residual.astype(BF16))).astype(BF16)))
    return out


def low_part(x):
    return jnp.where(low_half(x.shape), x, jnp.zeros_like(x))


def high_part(x):
    return jnp.where(low_half(x.shape), jnp.zeros_like(x), x)


def transitions(size, ats, v_ref, ops, solved_bufs):
    strict = iota((size, size), 0) > iota((size, size), 1)
    negs, sides = [], []
    for at in ats:
        keys, neg = grids(size, ops["from"], ops, at, strict)
        negs.append(neg)
        v = v_ref[:, at]
        values = diag2(high_part(swap_halves(v)), high_part(v))
        carried = mm(keys[0], values) + mm(keys[1], values)
        base = ops["from_start"][:, at]
        lows = cat([low_part(base), low_part(swap_halves(base))], 1)
        sides.append(split(lows + carried))
    found = inverses(negs, size)
    messages = []
    for at, x, side in zip(ats, found, sides):
        solved = split(mm(x[0], by_head(side[0])) + mm(x[0], by_head(side[1])) + mm(x[1], by_head(side[0])))
        wide = pl.ds(pl.multiple_of(2 * at.start, QUAD), QUAD)
        solved_bufs[0][:, wide] = solved[0]
        solved_bufs[1][:, wide] = solved[1]
        v = v_ref[:, at]
        ends = cat([ops["erase_end"][:, at], ops["key_end"][:, at]], 0)
        values = cat([high_part(swap_halves(v)), high_part(v)], 1)
        made = mm_tn(ends, cat([solved[0], values], 0)).astype(BF16)
        messages.append((made[:HEAD, :PAIR], made[HEAD:, PAIR:]))
    return messages


def readouts(size, at, v_ref, ops, solved_bufs, local_bufs):
    within = iota((size, size), 0) >= iota((size, size), 1)
    keys, erases = grids(size, ops["read"], ops, at, within)
    left = [cat([e[:, :PAIR], k[:, :PAIR], e[:, PAIR:], k[:, PAIR:]], 1) for k, e in zip(keys, erases)]
    wide = pl.ds(pl.multiple_of(2 * at.start, QUAD), QUAD)
    solved = solved_bufs[0][:, wide]
    v = v_ref[:, at]
    right = diag2(cat([solved[:, :PAIR], high_part(swap_halves(v))], 0), cat([solved[:, PAIR:], high_part(v)], 0))
    base = ops["read_start"][:, at]
    lows = cat([low_part(base), low_part(swap_halves(base))], 1)
    taken = mm(left[0], right) + mm(left[1], right) + mm(erases[0], by_head(solved_bufs[1][:, wide]))
    put_split(local_bufs, wide, lows + taken)


def mixer_kernel(devices, ranks, batch,
                 q_ref, k_ref, v_ref, low_ref, rate_ref, dup_ref, rup_ref, base_ref, gain_ref, w_ref,
                 out_ref,
                 from_high, from_low, read_high, read_low, key_high, key_low, erase_high, erase_low,
                 key_end, erase_end, from_start, read_start,
                 solved_high, solved_low, local_high, local_low, mix_buf,
                 message_buf, decay_buf, arrive_buf, arrive_decay, back_buf, start_buf, weight_buf, chain_buf,
                 message_sem, decay_sem, back_sem, sent_sem, sent_decay_sem, sent_back_sem,
                 right_sem, left_sem, cross_sem, mate_sem, sent_ring_sem, sent_cross_sem, sent_mate_sem, own_sem):
    size, width = q_ref.shape
    pairs = width // PAIR
    ops = {"from": (from_high, from_low), "read": (read_high, read_low), "key": (key_high, key_low),
           "erase": (erase_high, erase_low), "key_end": key_end, "erase_end": erase_end,
           "from_start": from_start, "read_start": read_start}
    solved_bufs = (solved_high, solved_low)
    local_bufs = (local_high, local_low)
    me = lax.axis_index("sp")
    rank = lax.axis_index("dp")
    length = ranks // 2
    half_way = length // 2
    core = lax.rem(rank, 2)
    line = rank // 2
    along = lambda step: lax.rem(line + step + length, length)
    at_rank = lambda row: {"dp": row * 2 + core}
    mate = {"dp": rank + 1 - 2 * core}
    x = lax.rem(me, XDIM)
    across = lambda step: {"sp": me - x + lax.rem(x + step + XDIM, XDIM)}
    parity = lax.rem(x, 2)
    rows = width // 2
    quarter = rows // 2

    barrier = pltpu.get_barrier_semaphore()

    @pl.loop(1, devices)
    def _(j):
        pl.semaphore_signal(barrier, inc=1, device_id={"sp": lax.rem(me + j, devices)}, device_id_type=MESH)

    for target in (at_rank(along(1)), at_rank(along(-1)), mate):
        pl.semaphore_signal(barrier, inc=1, device_id=target, device_id_type=MESH)
    own = pltpu.make_async_copy(w_ref, weight_buf.at[rank], own_sem)
    own.start()

    squashed = jnp.tanh(low_ref[...].astype(F32)).astype(BF16)
    rate_low = rate_ref[...]

    def prepare_quads(quads):
        for i in quads:
            prepare(size, pl.ds(pl.multiple_of(i * QUAD, QUAD), QUAD), q_ref, k_ref, squashed, rate_low,
                    dup_ref, rup_ref, base_ref, ops, decay_buf, i * 2)

    @pl.loop(0, pairs // batch)
    def _(b):
        prepare_quads([b * (batch // 2) + i for i in range(batch // 2)])

    pl.semaphore_wait(barrier, devices - 1 + 3)
    own.wait()

    piece = lambda source, start, count: weight_buf.at[
        source * 2 + core, pl.ds(pl.multiple_of(start, quarter), count)]

    def remote(ref, sem_out, sem_in, target):
        return pltpu.make_async_remote_copy(
            src_ref=ref, dst_ref=ref, send_sem=sem_out, recv_sem=sem_in, device_id=target, device_id_type=MESH)

    def ring(step, way):
        sign = 1 if way == 0 else -1
        source = along(-sign * (step - 1))
        if step < half_way:
            ref = piece(source, parity * rows, rows)
        else:
            ref = piece(source, parity * rows + way * quarter, quarter)
        sems = right_sem if way == 0 else left_sem
        return remote(ref, sent_ring_sem.at[way, step - 1], sems.at[step - 1], at_rank(along(sign)))

    def ring_arrival(step, way):
        sign = 1 if way == 0 else -1
        source = along(-sign * step)
        if step < half_way:
            ref = piece(source, parity * rows, rows)
        else:
            ref = piece(source, parity * rows + way * quarter, quarter)
        sems = right_sem if way == 0 else left_sem
        return remote(ref, sent_ring_sem.at[way, step - 1], sems.at[step - 1], at_rank(along(sign)))

    def cross(offset, way):
        source = along(offset)
        ref = piece(source, parity * rows + way * quarter, quarter)
        index = (offset + length) % length
        return remote(ref, sent_cross_sem.at[way, index], cross_sem.at[way, index], across(1 if way == 0 else -1))

    def cross_arrival(offset, way):
        source = along(offset)
        ref = piece(source, (1 - parity) * rows + way * quarter, quarter)
        index = (offset + length) % length
        return remote(ref, sent_cross_sem.at[way, index], cross_sem.at[way, index], across(1 if way == 0 else -1))

    def to_mate(offset, which):
        source = along(offset)
        index = (offset + length) % length
        start = (parity if which == 0 else 1 - parity) * rows
        return remote(piece(source, start, rows), sent_mate_sem.at[which, index], mate_sem.at[which, index], mate)

    def from_mate(offset, which):
        index = (offset + length) % length
        start = (parity if which == 0 else 1 - parity) * rows
        ref = weight_buf.at[along(offset) * 2 + 1 - core, pl.ds(pl.multiple_of(start, quarter), rows)]
        return remote(ref, sent_mate_sem.at[which, index], mate_sem.at[which, index], mate)

    def offsets(step):
        return [half_way] if step == half_way else [-step, step]

    for way in range(2):
        ring(1, way).start()
    for which in range(2):
        to_mate(0, which).start()

    def serve_ring(step):
        for way in range(2):
            ring_arrival(step, way).wait_recv()
            if step < half_way:
                ring(step + 1, way).start()
        for offset in offsets(step):
            for way in range(2):
                cross(offset, way).start()
            to_mate(offset, 0).start()

    served = set()

    def serve_cross(step):
        served.add(step)
        for offset in offsets(step):
            for way in range(2):
                cross_arrival(offset, way).wait_recv()
            to_mate(offset, 1).start()

    def head_copy(head, sender, target):
        return pltpu.make_async_remote_copy(
            src_ref=message_buf.at[head], dst_ref=arrive_buf.at[sender], send_sem=sent_sem, recv_sem=message_sem,
            device_id=target, device_id_type=MESH)

    def decay_copy(head, sender, target):
        return pltpu.make_async_remote_copy(
            src_ref=decay_buf.at[head], dst_ref=arrive_decay.at[sender], send_sem=sent_decay_sem,
            recv_sem=decay_sem, device_id=target, device_id_type=MESH)

    @pl.loop(0, pairs // batch)
    def _(b):
        ats = [pl.ds(pl.multiple_of((b * batch + i) * PAIR, PAIR), PAIR) for i in range(batch)]
        messages = transitions(size, ats, v_ref, ops, solved_bufs)
        for i, (first, second) in enumerate(messages):
            message_buf[2 * (b * batch + i)] = first
            message_buf[2 * (b * batch + i) + 1] = second
        count = 2 * batch

        @pl.loop(0, count)
        def _(j):
            head = b * count + lax.rem(me + j, count)

            @pl.when(head != me)
            def _():
                head_copy(head, me, {"sp": head}).start()
                decay_copy(head, me, {"sp": head}).start()

    arrive_buf[me] = message_buf[me]
    arrive_decay[me] = decay_buf[me]
    serve_ring(1)

    @pl.loop(0, pairs // batch)
    def _(b):
        for i in range(batch):
            readouts(size, pl.ds(pl.multiple_of((b * batch + i) * PAIR, PAIR), PAIR), v_ref, ops, solved_bufs,
                     local_bufs)

    serve_cross(1)
    if half_way > 1:
        serve_ring(2)

    others = pl.ds(0, devices - 1)
    pltpu.make_async_copy(arrive_buf.at[others], arrive_buf.at[others], message_sem).wait()
    pltpu.make_async_copy(arrive_decay.at[others], arrive_decay.at[others], decay_sem).wait()

    def back_copy(chunk, head, target):
        return pltpu.make_async_remote_copy(
            src_ref=back_buf.at[chunk], dst_ref=start_buf.at[head], send_sem=sent_back_sem, recv_sem=back_sem.at[head],
            device_id=target, device_id_type=MESH)

    row = iota((HEAD, PAIR), 0)
    lane = iota((HEAD, PAIR), 1)
    marker = jnp.where(lane == row + HEAD, F32(1.0), F32(0.0)).astype(BF16)
    lower = lane < HEAD

    chain_buf[...] = jnp.zeros_like(chain_buf)

    @pl.loop(0, devices)
    def _(c):
        state = chain_buf[...]
        average = jnp.mean(state, axis=0, keepdims=True)
        centred = jnp.where(lower, state - average, 0.0)
        packed = centred[: HEAD // 2] + pltpu.roll(centred[HEAD // 2 :], HEAD, 1)
        back_buf[c] = packed.astype(BF16)

        @pl.when(c != me)
        def _():
            back_copy(c, me, {"sp": c}).start()

        message = arrive_buf[c]
        left = jnp.where(lower, state.astype(BF16), marker)
        moved = mm_nt(left, cat([message, jnp.zeros_like(message)], 0))
        chain_buf[...] = moved + state * arrive_decay[c]

    start_buf[me] = back_buf[me]

    if half_way > 1:
        serve_cross(2)
    for step in range(3, half_way + 1):
        serve_ring(step)
        if step < half_way:
            serve_cross(step)

    mean_ones = cat([same_head_ones(PAIR, 1.0 / HEAD)] * 2, 0)
    centring = jnp.where(lane == row + HEAD, F32(1.0 - 1.0 / HEAD), F32(-1.0 / HEAD)).astype(BF16)

    def finish_pair(p):
        at = pl.ds(pl.multiple_of(p * PAIR, PAIR), PAIR)
        wide = pl.ds(pl.multiple_of(p * QUAD, QUAD), QUAD)
        rights = []
        for i in range(2):
            head = 2 * p + i

            @pl.when(head != me)
            def _():
                back_copy(me, head, {"sp": me}).wait_recv()

            packed = start_buf[head]
            rights.append(jnp.where(lower, cat([packed, swap_halves(packed)], 0), centring))
        right = diag2(rights[0], rights[1])
        centred = mm_nt(local_high[:, wide], right) + mm_nt(local_low[:, wide], right)
        variance = mm(cat(split(centred * centred), 1), mean_ones)
        mix_buf[:, at] = (centred * lax.rsqrt(variance + 1.0) * gain_ref[:, at]).astype(BF16)

    @pl.loop(0, pairs // batch)
    def _(b):
        for i in range(batch):
            finish_pair(b * batch + i)

    def project(offset):
        at = along(offset)
        weight = cat([weight_buf[2 * at], weight_buf[2 * at + 1]], 1)
        out_ref[:, pl.ds(pl.multiple_of(at * QUAD, QUAD), QUAD)] = mm(mix_buf[...], weight).astype(BF16)

    for which in range(2):
        from_mate(0, which).wait_recv()
    project(0)
    for step in range(1, half_way + 1):
        if step not in served:
            serve_cross(step)
        for offset in offsets(step):
            for which in range(2):
                from_mate(offset, which).wait_recv()
            project(offset)

    pltpu.make_async_copy(message_buf.at[others], message_buf.at[others], sent_sem).wait()
    pltpu.make_async_copy(decay_buf.at[others], decay_buf.at[others], sent_decay_sem).wait()
    pltpu.make_async_copy(back_buf.at[others], back_buf.at[others], sent_back_sem).wait()
    for step in range(1, half_way + 1):
        for way in range(2):
            ring(step, way).wait_send()
        for offset in offsets(step):
            for way in range(2):
                cross(offset, way).wait_send()
            for which in range(2):
                to_mate(offset, which).wait_send()
    for which in range(2):
        to_mate(0, which).wait_send()


def per_device(devices, ranks, query_rows, key_rows, value_rows, decay_low, rate_low, decay_up, rate_up,
               decay_base, norm_gain, out_weight):
    size, width = query_rows.shape[1:]
    heads = width // HEAD
    batch = min(4, width // PAIR)
    length = ranks // 2
    half_way = length // 2
    vmem = pl.BlockSpec(memory_space=pltpu.VMEM)
    dma = pltpu.SemaphoreType.DMA
    wide = lambda lanes: pltpu.VMEM((size, lanes), BF16)
    out = pl.pallas_call(
        functools.partial(mixer_kernel, devices, ranks, batch),
        in_specs=[vmem] * 9 + [pl.BlockSpec(memory_space=pl.ANY)],
        out_specs=vmem,
        out_shape=jax.ShapeDtypeStruct((size, out_weight.shape[1] * ranks), BF16),
        scratch_shapes=[wide(width) for _ in range(10)] + [pltpu.VMEM((size, width), F32)] * 2
        + [wide(2 * width) for _ in range(4)] + [wide(width)] + [
            pltpu.VMEM((heads, HEAD, PAIR), BF16),
            pltpu.VMEM((heads, 1, PAIR), F32),
            pltpu.VMEM((devices, HEAD, PAIR), BF16),
            pltpu.VMEM((devices, 1, PAIR), F32),
            pltpu.VMEM((devices, HEAD // 2, PAIR), BF16),
            pltpu.VMEM((heads, HEAD // 2, PAIR), BF16),
            pltpu.VMEM((ranks,) + out_weight.shape, BF16),
            pltpu.VMEM((HEAD, PAIR), F32),
            dma, dma, dma((heads,)), dma, dma, dma,
            dma((half_way,)), dma((half_way,)), dma((2, length)), dma((2, length)),
            dma((2, half_way)), dma((2, length)), dma((2, length)), dma,
        ],
        compiler_params=pltpu.CompilerParams(
            collective_id=0, has_side_effects=True, vmem_limit_bytes=60 * 2**20),
        cost_estimate=pl.CostEstimate(flops=10**10, bytes_accessed=10**7, transcendentals=0),
        name="mixer",
    )(query_rows[0], key_rows[0], value_rows[0], decay_low[0], rate_low[0], decay_up, rate_up,
      decay_base[None], norm_gain[None], out_weight)
    return out[None]


def solution(mesh):
    in_specs = (
        P("dp", "sp", None),
        P("dp", "sp", None),
        P("dp", "sp", None),
        P("dp", "sp", None),
        P("dp", "sp", None),
        P(),
        P(),
        P(),
        P(),
        P(None, "dp"),
    )
    return jax.shard_map(
        functools.partial(per_device, mesh.shape["sp"], mesh.shape["dp"]),
        mesh=mesh, in_specs=in_specs, out_specs=P("dp", "sp", None), check_vma=False,
    )
```

time: 183 us -> 78.4 us (0.43)
  the two profiles are of different devices: /device:TPU:502 before, /device:TPU:1 now
where the time goes in v1:
time: 78.4 us; the launch traced here: 78.2 us
  Pallas kernels  76.3 us (97%)
  local copies, waits for them, and re-layouts  1.88 us (2%)
    pallas_call x1, Pallas kernels, per_device(): pl.pallas_call(functools.partial(mixer_kernel, devices, ranks, batch), in...  76.3 us
    unnamed x1, local copies, waits for them, and re-layouts  1.88 us

profile of v1, /device:TPU:1, one launch (start us, length us, event | category | flops | bytes accessed | tf_op | source)
XLA Modules:
  0.0 78.2 jit_solution(10899141958652233746)
XLA Ops:
  0.0 76.3 %mixer.1 = bf16[128,2048]{1,0:T(8,128)(2,1)} custom-call(bf16[128,2048]{1,0:T(8,128)(2,1)} %bitcast.9, bf16[128,2048]{1,0:T(8,128)(2,1)} %bitcast.10, bf16[128,2048]{1,0:T(8,128)(2,1)} %bitcast.11, bf16[128,128]{1,0:T(8,128)(2,1)} %bitcast.12, bf16[128,128]{1,0:T(8,128)(2,1)} %bitcast.13, bf16[128,2048]{1,0:T(8,128)(2,1)} %dup_ref.1, ...), custom_call_target="tpu_custom_call" | custom-call | flops 10000000000 | bytes 10000000 | tf_op jit(solution)/shard_map/mixer/pallas_call | solution.py:494
  76.3 1.9 %copy.12 = bf16[1,128,2048]{2,1,0:T(8,128)(2,1)} copy(bf16[1,128,2048]{2,1,0:T(8,128)(2,1)} %bitcast.8) | data formatting | bytes 1048576

commit v2 on v1

--- a/solution.py
+++ b/solution.py
@@ -211,7 +211,7 @@
                  from_high, from_low, read_high, read_low, key_high, key_low, erase_high, erase_low,
                  key_end, erase_end, from_start, read_start,
                  solved_high, solved_low, local_high, local_low, mix_buf,
-                 message_buf, decay_buf, arrive_buf, arrive_decay, back_buf, start_buf, weight_buf, chain_buf,
+                 message_buf, decay_buf, arrive_buf, arrive_decay, back_buf, start_buf, weight_buf,
                  message_sem, decay_sem, back_sem, sent_sem, sent_decay_sem, sent_back_sem,
                  right_sem, left_sem, cross_sem, mate_sem, sent_ring_sem, sent_cross_sem, sent_mate_sem, own_sem):
     size, width = q_ref.shape
@@ -236,6 +236,14 @@
     rows = width // 2
     quarter = rows // 2
 
+    planes = devices // XDIM
+    plane = me // XDIM
+    my_head = lax.rem(x + planes * XDIM - plane, XDIM) * planes + plane
+
+    def keeper(head):
+        place = lax.rem(head, planes)
+        return place * XDIM + lax.rem(place + head // planes, XDIM)
+
     barrier = pltpu.get_barrier_semaphore()
 
     @pl.loop(1, devices)
@@ -363,13 +371,13 @@
         def _(j):
             head = b * count + lax.rem(me + j, count)
 
-            @pl.when(head != me)
+            @pl.when(head != my_head)
             def _():
-                head_copy(head, me, {"sp": head}).start()
-                decay_copy(head, me, {"sp": head}).start()
-
-    arrive_buf[me] = message_buf[me]
-    arrive_decay[me] = decay_buf[me]
+                head_copy(head, me, {"sp": keeper(head)}).start()
+                decay_copy(head, me, {"sp": keeper(head)}).start()
+
+    arrive_buf[me] = message_buf[my_head]
+    arrive_decay[me] = decay_buf[my_head]
     serve_ring(1)
 
     @pl.loop(0, pairs // batch)
@@ -393,29 +401,55 @@
 
     row = iota((HEAD, PAIR), 0)
     lane = iota((HEAD, PAIR), 1)
+    lower = lane < HEAD
     marker = jnp.where(lane == row + HEAD, F32(1.0), F32(0.0)).astype(BF16)
-    lower = lane < HEAD
-
-    chain_buf[...] = jnp.zeros_like(chain_buf)
-
-    @pl.loop(0, devices)
-    def _(c):
-        state = chain_buf[...]
+    marker = cat([jnp.zeros_like(marker), marker], 0)
+    low_tall = iota((PAIR, PAIR), 1) < HEAD
+    begin = jnp.where(iota((PAIR, PAIR), 0) == iota((PAIR, PAIR), 1), F32(1.0), F32(0.0))
+    begin = jnp.where(low_tall, begin, 0.0)
+    per = devices // XDIM
+    steps = [[begin] for _ in range(XDIM)]
+    for r in range(per):
+        for g in range(XDIM):
+            if g == XDIM - 1 and r == per - 1:
+                continue
+            c = g * per + r
+            now = steps[g][-1]
+            message = arrive_buf[c]
+            moved = mm_nt(jnp.where(low_tall, now.astype(BF16), marker), cat([message, jnp.zeros_like(message)], 0))
+            steps[g].append(moved + now * arrive_decay[c])
+
+    def put_back(c, state):
         average = jnp.mean(state, axis=0, keepdims=True)
         centred = jnp.where(lower, state - average, 0.0)
-        packed = centred[: HEAD // 2] + pltpu.roll(centred[HEAD // 2 :], HEAD, 1)
-        back_buf[c] = packed.astype(BF16)
-
-        @pl.when(c != me)
-        def _():
-            back_copy(c, me, {"sp": c}).start()
-
-        message = arrive_buf[c]
-        left = jnp.where(lower, state.astype(BF16), marker)
-        moved = mm_nt(left, cat([message, jnp.zeros_like(message)], 0))
-        chain_buf[...] = moved + state * arrive_decay[c]
-
-    start_buf[me] = back_buf[me]
+        back_buf[c] = (centred[: HEAD // 2] + pltpu.roll(centred[HEAD // 2 :], HEAD, 1)).astype(BF16)
+
+    state = jnp.zeros((HEAD, PAIR), F32)
+    for g in range(XDIM):
+        high, low = split(state)
+        left = cat([jnp.where(lower, high, jnp.zeros_like(high)), jnp.where(lower, low, jnp.zeros_like(low))], 0)
+        for r in range(per + 1):
+            if g == XDIM - 1 and r == per:
+                continue
+            both = steps[g][r]
+            if r == 0:
+                reached = state
+            elif g == 0:
+                reached = both[HEAD:]
+            else:
+                moved = mm(left, both.astype(BF16))
+                reached = moved[:HEAD] + moved[HEAD:] + both[HEAD:]
+            if r < per:
+                put_back(g * per + r, reached)
+            else:
+                state = reached
+
+    @pl.loop(1, devices)
+    def _(j):
+        chunk = lax.rem(me + j, devices)
+        back_copy(chunk, my_head, {"sp": chunk}).start()
+
+    start_buf[my_head] = back_buf[me]
 
     if half_way > 1:
         serve_cross(2)
@@ -434,7 +468,7 @@
         for i in range(2):
             head = 2 * p + i
 
-            @pl.when(head != me)
+            @pl.when(head != my_head)
             def _():
                 back_copy(me, head, {"sp": me}).wait_recv()
 
@@ -464,6 +498,7 @@
         for offset in offsets(step):
             for which in range(2):
                 from_mate(offset, which).wait_recv()
+        for offset in offsets(step):
             project(offset)
 
     pltpu.make_async_copy(message_buf.at[others], message_buf.at[others], sent_sem).wait()
@@ -505,7 +540,6 @@
             pltpu.VMEM((devices, HEAD // 2, PAIR), BF16),
             pltpu.VMEM((heads, HEAD // 2, PAIR), BF16),
             pltpu.VMEM((ranks,) + out_weight.shape, BF16),
-            pltpu.VMEM((HEAD, PAIR), F32),
             dma, dma, dma((heads,)), dma, dma, dma,
             dma((half_way,)), dma((half_way,)), dma((2, length)), dma((2, length)),
             dma((2, half_way)), dma((2, length)), dma((2, length)), dma,

time: 78.4 us -> 82.3 us (1.050)
  Pallas kernels: 76.3 us -> 79.5 us
    pallas_call x1, Pallas kernels: 76.3 us -> 79.5 us  [per_device(): pl.pallas_call(functools.partial(mixer_kernel, devices, ranks, batch), in...]
where the time goes in v2:
time: 82.3 us; the launch traced here: 81.4 us
  Pallas kernels  79.5 us (97%)
  local copies, waits for them, and re-layouts  1.88 us (2%)
    pallas_call x1, Pallas kernels, per_device(): pl.pallas_call(functools.partial(mixer_kernel, devices, ranks, batch), in...  79.5 us
    unnamed x1, local copies, waits for them, and re-layouts  1.88 us

profile of v2, /device:TPU:1, one launch (start us, length us, event | category | flops | bytes accessed | tf_op | source)
XLA Modules:
  0.0 81.4 jit_solution(501651589737101079)
XLA Ops:
  0.0 79.5 %mixer.1 = bf16[128,2048]{1,0:T(8,128)(2,1)} custom-call(bf16[128,2048]{1,0:T(8,128)(2,1)} %bitcast.9, bf16[128,2048]{1,0:T(8,128)(2,1)} %bitcast.10, bf16[128,2048]{1,0:T(8,128)(2,1)} %bitcast.11, bf16[128,128]{1,0:T(8,128)(2,1)} %bitcast.12, bf16[128,128]{1,0:T(8,128)(2,1)} %bitcast.13, bf16[128,2048]{1,0:T(8,128)(2,1)} %dup_ref.1, ...), custom_call_target="tpu_custom_call" | custom-call | flops 10000000000 | bytes 10000000 | tf_op jit(solution)/shard_map/mixer/pallas_call | solution.py:529
  79.5 1.9 %copy.12 = bf16[1,128,2048]{2,1,0:T(8,128)(2,1)} copy(bf16[1,128,2048]{2,1,0:T(8,128)(2,1)} %bitcast.8) | data formatting | bytes 1048576

commit v3 on v2

--- a/solution.py
+++ b/solution.py
@@ -263,13 +263,6 @@
             prepare(size, pl.ds(pl.multiple_of(i * QUAD, QUAD), QUAD), q_ref, k_ref, squashed, rate_low,
                     dup_ref, rup_ref, base_ref, ops, decay_buf, i * 2)
 
-    @pl.loop(0, pairs // batch)
-    def _(b):
-        prepare_quads([b * (batch // 2) + i for i in range(batch // 2)])
-
-    pl.semaphore_wait(barrier, devices - 1 + 3)
-    own.wait()
-
     piece = lambda source, start, count: weight_buf.at[
         source * 2 + core, pl.ds(pl.multiple_of(start, quarter), count)]
 
@@ -324,11 +317,6 @@
     def offsets(step):
         return [half_way] if step == half_way else [-step, step]
 
-    for way in range(2):
-        ring(1, way).start()
-    for which in range(2):
-        to_mate(0, which).start()
-
     def serve_ring(step):
         for way in range(2):
             ring_arrival(step, way).wait_recv()
@@ -348,6 +336,19 @@
                 cross_arrival(offset, way).wait_recv()
             to_mate(offset, 1).start()
 
+    @pl.loop(0, pairs // batch)
+    def _(b):
+        prepare_quads([b * (batch // 2) + i for i in range(batch // 2)])
+
+        @pl.when(b == 0)
+        def _():
+            pl.semaphore_wait(barrier, devices - 1 + 3)
+            own.wait()
+            for way in range(2):
+                ring(1, way).start()
+            for which in range(2):
+                to_mate(0, which).start()
+
     def head_copy(head, sender, target):
         return pltpu.make_async_remote_copy(
             src_ref=message_buf.at[head], dst_ref=arrive_buf.at[sender], send_sem=sent_sem, recv_sem=message_sem,
@@ -376,9 +377,15 @@
                 head_copy(head, me, {"sp": keeper(head)}).start()
                 decay_copy(head, me, {"sp": keeper(head)}).start()
 
+        @pl.when(b == 0)
+        def _():
+            serve_ring(1)
+
     arrive_buf[me] = message_buf[my_head]
     arrive_decay[me] = decay_buf[my_head]
-    serve_ring(1)
+    serve_cross(1)
+    if half_way > 1:
+        serve_ring(2)
 
     @pl.loop(0, pairs // batch)
     def _(b):
@@ -386,9 +393,10 @@
             readouts(size, pl.ds(pl.multiple_of((b * batch + i) * PAIR, PAIR), PAIR), v_ref, ops, solved_bufs,
                      local_bufs)
 
-    serve_cross(1)
     if half_way > 1:
-        serve_ring(2)
+        serve_cross(2)
+    if half_way > 2:
+        serve_ring(3)
 
     others = pl.ds(0, devices - 1)
     pltpu.make_async_copy(arrive_buf.at[others], arrive_buf.at[others], message_sem).wait()
@@ -451,28 +459,27 @@
 
     start_buf[my_head] = back_buf[me]
 
-    if half_way > 1:
-        serve_cross(2)
-    for step in range(3, half_way + 1):
-        serve_ring(step)
-        if step < half_way:
-            serve_cross(step)
+    for step in range(3, half_way):
+        serve_cross(step)
+        serve_ring(step + 1)
 
     mean_ones = cat([same_head_ones(PAIR, 1.0 / HEAD)] * 2, 0)
     centring = jnp.where(lane == row + HEAD, F32(1.0 - 1.0 / HEAD), F32(-1.0 / HEAD)).astype(BF16)
+
+    def finish_wait(p):
+        for i in range(2):
+            head = 2 * p + i
+
+            @pl.when(head != my_head)
+            def _():
+                back_copy(me, head, {"sp": me}).wait_recv()
 
     def finish_pair(p):
         at = pl.ds(pl.multiple_of(p * PAIR, PAIR), PAIR)
         wide = pl.ds(pl.multiple_of(p * QUAD, QUAD), QUAD)
         rights = []
         for i in range(2):
-            head = 2 * p + i
-
-            @pl.when(head != my_head)
-            def _():
-                back_copy(me, head, {"sp": me}).wait_recv()
-
-            packed = start_buf[head]
+            packed = start_buf[2 * p + i]
             rights.append(jnp.where(lower, cat([packed, swap_halves(packed)], 0), centring))
         right = diag2(rights[0], rights[1])
         centred = mm_nt(local_high[:, wide], right) + mm_nt(local_low[:, wide], right)
@@ -482,6 +489,8 @@
     @pl.loop(0, pairs // batch)
     def _(b):
         for i in range(batch):
+            finish_wait(b * batch + i)
+        for i in range(batch):
             finish_pair(b * batch + i)
 
     def project(offset):
@@ -489,17 +498,18 @@
         weight = cat([weight_buf[2 * at], weight_buf[2 * at + 1]], 1)
         out_ref[:, pl.ds(pl.multiple_of(at * QUAD, QUAD), QUAD)] = mm(mix_buf[...], weight).astype(BF16)
 
+    last = [step for step in range(1, half_way + 1) if step not in served]
+    early = [offset for step in range(1, half_way) for offset in offsets(step)]
+    for offset in [0] + early:
+        for which in range(2):
+            from_mate(offset, which).wait_recv()
+    for step in last:
+        serve_cross(step)
+    for offset in [0] + early:
+        project(offset)
     for which in range(2):
-        from_mate(0, which).wait_recv()
-    project(0)
-    for step in range(1, half_way + 1):
-        if step not in served:
-            serve_cross(step)
-        for offset in offsets(step):
-            for which in range(2):
-                from_mate(offset, which).wait_recv()
-        for offset in offsets(step):
-            project(offset)
+        from_mate(half_way, which).wait_recv()
+    project(half_way)
 
     pltpu.make_async_copy(message_buf.at[others], message_buf.at[others], sent_sem).wait()
     pltpu.make_async_copy(decay_buf.at[others], decay_buf.at[others], sent_decay_sem).wait()
@@ -520,7 +530,7 @@
                decay_base, norm_gain, out_weight):
     size, width = query_rows.shape[1:]
     heads = width // HEAD
-    batch = min(4, width // PAIR)
+    batch = min(8, width // PAIR)
     length = ranks // 2
     half_way = length // 2
     vmem = pl.BlockSpec(memory_space=pltpu.VMEM)

time: 82.3 us -> 69.2 us (0.84)
  Pallas kernels: 79.5 us -> 67.2 us
    pallas_call x1, Pallas kernels: 79.5 us -> 67.2 us  [per_device(): pl.pallas_call(functools.partial(mixer_kernel, devices, ranks, batch), in...]
where the time goes in v3:
time: 69.2 us; the launch traced here: 69.1 us
  Pallas kernels  67.2 us (97%)
  local copies, waits for them, and re-layouts  1.88 us (3%)
    pallas_call x1, Pallas kernels, per_device(): pl.pallas_call(functools.partial(mixer_kernel, devices, ranks, batch), in...  67.2 us
    unnamed x1, local copies, waits for them, and re-layouts  1.88 us

profile of v3, /device:TPU:1, one launch (start us, length us, event | category | flops | bytes accessed | tf_op | source)
XLA Modules:
  0.0 69.1 jit_solution(12691214426187842081)
XLA Ops:
  0.0 67.2 %mixer.1 = bf16[128,2048]{1,0:T(8,128)(2,1)} custom-call(bf16[128,2048]{1,0:T(8,128)(2,1)} %bitcast.9, bf16[128,2048]{1,0:T(8,128)(2,1)} %bitcast.10, bf16[128,2048]{1,0:T(8,128)(2,1)} %bitcast.11, bf16[128,128]{1,0:T(8,128)(2,1)} %bitcast.12, bf16[128,128]{1,0:T(8,128)(2,1)} %bitcast.13, bf16[128,2048]{1,0:T(8,128)(2,1)} %dup_ref.1, ...), custom_call_target="tpu_custom_call" | custom-call | flops 10000000000 | bytes 10000000 | tf_op jit(solution)/shard_map/mixer/pallas_call | solution.py:539
  67.2 1.9 %copy.12 = bf16[1,128,2048]{2,1,0:T(8,128)(2,1)} copy(bf16[1,128,2048]{2,1,0:T(8,128)(2,1)} %bitcast.8) | data formatting | bytes 1048576

commit v4 on v3

--- a/solution.py
+++ b/solution.py
@@ -72,25 +72,40 @@
     refs[1][:, at] = low
 
 
+def wavefront(works):
+    running = []
+    waiting = list(works)
+    while waiting or running:
+        if waiting:
+            running.append(waiting.pop(0))
+        running = [work for work in running if next(work, 0) is None]
+
+
 def prepare(size, at, q_ref, k_ref, squashed, rate_low, dup_ref, rup_ref, base_ref, ops, decay_buf, pair):
     middle = size // 2
     upto = jnp.where(iota((size, size), 0) >= iota((size, size), 1), F32(1.0), F32(0.0)).astype(BF16)
     upto = cat([upto, upto], 1)
-    decay_pre = (base_ref[:, at] + mm(squashed, dup_ref[:, at])).astype(BF16).astype(F32)
-    rate_pre = mm(rate_low, rup_ref[:, at]).astype(BF16).astype(F32)
+    decay_pre = mm(squashed, dup_ref[:, at])
+    rate_pre = mm(rate_low, rup_ref[:, at])
+    yield
+    decay_pre = (base_ref[:, at] + decay_pre).astype(BF16).astype(F32)
+    rate_pre = rate_pre.astype(BF16).astype(F32)
     log_decay = -math.exp(-0.5) / (1.0 + jnp.exp(-decay_pre))
     rate = 1.0 / (1.0 + jnp.exp(-rate_pre))
     running = mm(upto, cat(split(log_decay), 0))
+    k = k_ref[:, at].astype(F32)
+    norm = mm(cat(split(k * k), 1), cat([same_head_ones(QUAD, 1.0)] * 2, 0))
+    yield
     centre = running[middle : middle + 1]
     final = running[size - 1 :]
-    ahead = jnp.exp(running - centre)
-    before = jnp.exp(running - log_decay - centre)
-    behind = jnp.exp(centre - running)
+    shifted = running - centre
+    ahead = jnp.exp(shifted)
+    before = jnp.exp(shifted - log_decay)
+    behind = jnp.exp(-shifted)
     at_centre = jnp.exp(centre)
     at_end = jnp.exp(final - centre)
-    k = k_ref[:, at].astype(F32)
     q = q_ref[:, at].astype(F32)
-    unit = k * lax.rsqrt(1.0 + mm(cat(split(k * k), 1), cat([same_head_ones(QUAD, 1.0)] * 2, 0)))
+    unit = k * lax.rsqrt(1.0 + norm)
     erase_from = unit * before
     read_mid = q * ahead
     key_to = k * behind
@@ -114,11 +129,14 @@
     return diag2(x[:, :PAIR], x[:, PAIR:])
 
 
-def grids(size, left, ops, at, keep):
+def raw_grid(left, ops, at):
     high, low = (stack_pair(ref[:, at]) for ref in left)
     right = cat([ops["key"][0][:, at], ops["erase"][0][:, at]], 0)
     rest = cat([ops["key"][1][:, at], ops["erase"][1][:, at]], 0)
-    grid = mm_nt(cat([high, low], 1), cat([right, right], 1)) + mm_nt(high, rest)
+    return mm_nt(cat([high, low], 1), cat([right, right], 1)) + mm_nt(high, rest)
+
+
+def grid_parts(size, grid, keep):
     part = lambda i, j: jnp.where(keep, grid[i * size : (i + 1) * size, j * size : (j + 1) * size], 0.0)
     return split(cat([part(0, 0), part(1, 0)], 1)), split(cat([part(0, 1), part(1, 1)], 1))
 
@@ -149,11 +167,9 @@
             step = [mm(take(x), by_head(y)).astype(BF16) for x, y in zip(found, right)]
             found = [x + spread(t) for x, t in zip(found, step)]
         block *= 2
-    out = []
-    for (high, low), x in zip(splits, found):
-        residual = (eye - x).astype(F32) + (mm(high, by_head(x)) + mm(low, by_head(x)))
-        out.append((x, mm(x, by_head(residual.astype(BF16))).astype(BF16)))
-    return out
+    left = [mm(high, by_head(x)) + mm(low, by_head(x)) for (high, low), x in zip(splits, found)]
+    left = [((eye - x).astype(F32) + r).astype(BF16) for x, r in zip(found, left)]
+    return [(x, mm(x, by_head(r)).astype(BF16)) for x, r in zip(found, left)]
 
 
 def low_part(x):
@@ -167,41 +183,50 @@
 def transitions(size, ats, v_ref, ops, solved_bufs):
     strict = iota((size, size), 0) > iota((size, size), 1)
     negs, sides = [], []
-    for at in ats:
-        keys, neg = grids(size, ops["from"], ops, at, strict)
+
+    def front(at):
+        grid = raw_grid(ops["from"], ops, at)
+        yield
+        keys, neg = grid_parts(size, grid, strict)
         negs.append(neg)
         v = v_ref[:, at]
         values = diag2(high_part(swap_halves(v)), high_part(v))
         carried = mm(keys[0], values) + mm(keys[1], values)
+        yield
         base = ops["from_start"][:, at]
         lows = cat([low_part(base), low_part(swap_halves(base))], 1)
         sides.append(split(lows + carried))
+
+    wavefront([front(at) for at in ats])
     found = inverses(negs, size)
-    messages = []
-    for at, x, side in zip(ats, found, sides):
-        solved = split(mm(x[0], by_head(side[0])) + mm(x[0], by_head(side[1])) + mm(x[1], by_head(side[0])))
+    solved = [split(mm(x[0], by_head(side[0])) + mm(x[0], by_head(side[1])) + mm(x[1], by_head(side[0])))
+              for x, side in zip(found, sides)]
+    made = []
+    for at, parts in zip(ats, solved):
         wide = pl.ds(pl.multiple_of(2 * at.start, QUAD), QUAD)
-        solved_bufs[0][:, wide] = solved[0]
-        solved_bufs[1][:, wide] = solved[1]
+        solved_bufs[0][:, wide] = parts[0]
+        solved_bufs[1][:, wide] = parts[1]
         v = v_ref[:, at]
         ends = cat([ops["erase_end"][:, at], ops["key_end"][:, at]], 0)
         values = cat([high_part(swap_halves(v)), high_part(v)], 1)
-        made = mm_tn(ends, cat([solved[0], values], 0)).astype(BF16)
-        messages.append((made[:HEAD, :PAIR], made[HEAD:, PAIR:]))
-    return messages
+        made.append(mm_tn(ends, cat([parts[0], values], 0)))
+    return [(m[:HEAD, :PAIR].astype(BF16), m[HEAD:, PAIR:].astype(BF16)) for m in made]
 
 
 def readouts(size, at, v_ref, ops, solved_bufs, local_bufs):
     within = iota((size, size), 0) >= iota((size, size), 1)
-    keys, erases = grids(size, ops["read"], ops, at, within)
+    grid = raw_grid(ops["read"], ops, at)
+    yield
+    keys, erases = grid_parts(size, grid, within)
     left = [cat([e[:, :PAIR], k[:, :PAIR], e[:, PAIR:], k[:, PAIR:]], 1) for k, e in zip(keys, erases)]
     wide = pl.ds(pl.multiple_of(2 * at.start, QUAD), QUAD)
     solved = solved_bufs[0][:, wide]
     v = v_ref[:, at]
     right = diag2(cat([solved[:, :PAIR], high_part(swap_halves(v))], 0), cat([solved[:, PAIR:], high_part(v)], 0))
+    taken = mm(left[0], right) + mm(left[1], right) + mm(erases[0], by_head(solved_bufs[1][:, wide]))
+    yield
     base = ops["read_start"][:, at]
     lows = cat([low_part(base), low_part(swap_halves(base))], 1)
-    taken = mm(left[0], right) + mm(left[1], right) + mm(erases[0], by_head(solved_bufs[1][:, wide]))
     put_split(local_bufs, wide, lows + taken)
 
 
@@ -259,9 +284,8 @@
     rate_low = rate_ref[...]
 
     def prepare_quads(quads):
-        for i in quads:
-            prepare(size, pl.ds(pl.multiple_of(i * QUAD, QUAD), QUAD), q_ref, k_ref, squashed, rate_low,
-                    dup_ref, rup_ref, base_ref, ops, decay_buf, i * 2)
+        wavefront([prepare(size, pl.ds(pl.multiple_of(i * QUAD, QUAD), QUAD), q_ref, k_ref, squashed, rate_low,
+                           dup_ref, rup_ref, base_ref, ops, decay_buf, i * 2) for i in quads])
 
     piece = lambda source, start, count: weight_buf.at[
         source * 2 + core, pl.ds(pl.multiple_of(start, quarter), count)]
@@ -389,9 +413,8 @@
 
     @pl.loop(0, pairs // batch)
     def _(b):
-        for i in range(batch):
-            readouts(size, pl.ds(pl.multiple_of((b * batch + i) * PAIR, PAIR), PAIR), v_ref, ops, solved_bufs,
-                     local_bufs)
+        wavefront([readouts(size, pl.ds(pl.multiple_of((b * batch + i) * PAIR, PAIR), PAIR), v_ref, ops,
+                            solved_bufs, local_bufs) for i in range(batch)])
 
     if half_way > 1:
         serve_cross(2)
@@ -483,15 +506,16 @@
             rights.append(jnp.where(lower, cat([packed, swap_halves(packed)], 0), centring))
         right = diag2(rights[0], rights[1])
         centred = mm_nt(local_high[:, wide], right) + mm_nt(local_low[:, wide], right)
+        yield
         variance = mm(cat(split(centred * centred), 1), mean_ones)
+        yield
         mix_buf[:, at] = (centred * lax.rsqrt(variance + 1.0) * gain_ref[:, at]).astype(BF16)
 
     @pl.loop(0, pairs // batch)
     def _(b):
         for i in range(batch):
             finish_wait(b * batch + i)
-        for i in range(batch):
-            finish_pair(b * batch + i)
+        wavefront([finish_pair(b * batch + i) for i in range(batch)])
 
     def project(offset):
         at = along(offset)

time: 69.2 us -> 64.8 us (0.936)
  Pallas kernels: 67.2 us -> 62.3 us
    pallas_call x1, Pallas kernels: 67.2 us -> 62.3 us  [per_device(): pl.pallas_call(functools.partial(mixer_kernel, devices, ranks, batch), in...]
where the time goes in v4:
time: 64.8 us; the launch traced here: 64.2 us
  Pallas kernels  62.3 us (96%)
  local copies, waits for them, and re-layouts  1.88 us (3%)
    pallas_call x1, Pallas kernels, per_device(): pl.pallas_call(functools.partial(mixer_kernel, devices, ranks, batch), in...  62.3 us
    unnamed x1, local copies, waits for them, and re-layouts  1.88 us

profile of v4, /device:TPU:1, one launch (start us, length us, event | category | flops | bytes accessed | tf_op | source)
XLA Modules:
  0.0 64.2 jit_solution(15659267027731128917)
XLA Ops:
  0.0 62.3 %mixer.1 = bf16[128,2048]{1,0:T(8,128)(2,1)} custom-call(bf16[128,2048]{1,0:T(8,128)(2,1)} %bitcast.9, bf16[128,2048]{1,0:T(8,128)(2,1)} %bitcast.10, bf16[128,2048]{1,0:T(8,128)(2,1)} %bitcast.11, bf16[128,128]{1,0:T(8,128)(2,1)} %bitcast.12, bf16[128,128]{1,0:T(8,128)(2,1)} %bitcast.13, bf16[128,2048]{1,0:T(8,128)(2,1)} %dup_ref.1, ...), custom_call_target="tpu_custom_call" | custom-call | flops 10000000000 | bytes 10000000 | tf_op jit(solution)/shard_map/mixer/pallas_call | solution.py:563
  62.3 1.9 %copy.12 = bf16[1,128,2048]{2,1,0:T(8,128)(2,1)} copy(bf16[1,128,2048]{2,1,0:T(8,128)(2,1)} %bitcast.8) | data formatting | bytes 1048576

commit v5 on v4

--- a/solution.py
+++ b/solution.py
@@ -180,7 +180,7 @@
     return jnp.where(low_half(x.shape), jnp.zeros_like(x), x)
 
 
-def transitions(size, ats, v_ref, ops, solved_bufs):
+def transitions(size, ats, v_ref, ops, solved_bufs, pause):
     strict = iota((size, size), 0) > iota((size, size), 1)
     negs, sides = [], []
 
@@ -199,6 +199,7 @@
 
     wavefront([front(at) for at in ats])
     found = inverses(negs, size)
+    pause()
     solved = [split(mm(x[0], by_head(side[0])) + mm(x[0], by_head(side[1])) + mm(x[1], by_head(side[0])))
               for x, side in zip(found, sides)]
     made = []
@@ -231,14 +232,16 @@
 
 
 def mixer_kernel(devices, ranks, batch,
-                 q_ref, k_ref, v_ref, low_ref, rate_ref, dup_ref, rup_ref, base_ref, gain_ref, w_ref,
+                 q_in, k_in, v_in, low_ref, rate_ref, dup_in, rup_in, base_ref, gain_ref, w_ref,
                  out_ref,
+                 q_ref, k_ref, v_ref, dup_ref, rup_ref, load_sem,
                  from_high, from_low, read_high, read_low, key_high, key_low, erase_high, erase_low,
                  key_end, erase_end, from_start, read_start,
                  solved_high, solved_low, local_high, local_low, mix_buf,
                  message_buf, decay_buf, arrive_buf, arrive_decay, back_buf, start_buf, weight_buf,
                  message_sem, decay_sem, back_sem, sent_sem, sent_decay_sem, sent_back_sem,
-                 right_sem, left_sem, cross_sem, mate_sem, sent_ring_sem, sent_cross_sem, sent_mate_sem, own_sem):
+                 ring_sem, cross_sem, mate_sem, whole_sem, sent_ring_sem, sent_cross_sem, sent_mate_sem, sent_whole_sem,
+                 own_sem):
     size, width = q_ref.shape
     pairs = width // PAIR
     ops = {"from": (from_high, from_low), "read": (read_high, read_low), "key": (key_high, key_low),
@@ -269,6 +272,13 @@
         place = lax.rem(head, planes)
         return place * XDIM + lax.rem(place + head // planes, XDIM)
 
+    own = pltpu.make_async_copy(w_ref, weight_buf.at[rank], own_sem)
+    own.start()
+    loads = [pltpu.make_async_copy(source, target, load_sem.at[i]) for i, (source, target) in enumerate(
+        ((dup_in, dup_ref), (rup_in, rup_ref), (k_in, k_ref), (q_in, q_ref), (v_in, v_ref)))]
+    for load in loads:
+        load.start()
+
     barrier = pltpu.get_barrier_semaphore()
 
     @pl.loop(1, devices)
@@ -277,101 +287,94 @@
 
     for target in (at_rank(along(1)), at_rank(along(-1)), mate):
         pl.semaphore_signal(barrier, inc=1, device_id=target, device_id_type=MESH)
-    own = pltpu.make_async_copy(w_ref, weight_buf.at[rank], own_sem)
-    own.start()
-
-    squashed = jnp.tanh(low_ref[...].astype(F32)).astype(BF16)
-    rate_low = rate_ref[...]
-
-    def prepare_quads(quads):
-        wavefront([prepare(size, pl.ds(pl.multiple_of(i * QUAD, QUAD), QUAD), q_ref, k_ref, squashed, rate_low,
-                           dup_ref, rup_ref, base_ref, ops, decay_buf, i * 2) for i in quads])
-
-    piece = lambda source, start, count: weight_buf.at[
-        source * 2 + core, pl.ds(pl.multiple_of(start, quarter), count)]
+
+    last = 2 * half_way - 2
+
+    def quarters(source, kind, start):
+        return weight_buf.at[source * 2 + kind, pl.ds(pl.multiple_of(start, quarter), quarter)]
 
     def remote(ref, sem_out, sem_in, target):
         return pltpu.make_async_remote_copy(
             src_ref=ref, dst_ref=ref, send_sem=sem_out, recv_sem=sem_in, device_id=target, device_id_type=MESH)
 
-    def ring(step, way):
-        sign = 1 if way == 0 else -1
-        source = along(-sign * (step - 1))
-        if step < half_way:
-            ref = piece(source, parity * rows, rows)
-        else:
-            ref = piece(source, parity * rows + way * quarter, quarter)
-        sems = right_sem if way == 0 else left_sem
-        return remote(ref, sent_ring_sem.at[way, step - 1], sems.at[step - 1], at_rank(along(sign)))
-
-    def ring_arrival(step, way):
-        sign = 1 if way == 0 else -1
-        source = along(-sign * step)
-        if step < half_way:
-            ref = piece(source, parity * rows, rows)
-        else:
-            ref = piece(source, parity * rows + way * quarter, quarter)
-        sems = right_sem if way == 0 else left_sem
-        return remote(ref, sent_ring_sem.at[way, step - 1], sems.at[step - 1], at_rank(along(sign)))
-
-    def cross(offset, way):
-        source = along(offset)
-        ref = piece(source, parity * rows + way * quarter, quarter)
-        index = (offset + length) % length
-        return remote(ref, sent_cross_sem.at[way, index], cross_sem.at[way, index], across(1 if way == 0 else -1))
-
-    def cross_arrival(offset, way):
-        source = along(offset)
-        ref = piece(source, (1 - parity) * rows + way * quarter, quarter)
-        index = (offset + length) % length
-        return remote(ref, sent_cross_sem.at[way, index], cross_sem.at[way, index], across(1 if way == 0 else -1))
-
-    def to_mate(offset, which):
-        source = along(offset)
-        index = (offset + length) % length
-        start = (parity if which == 0 else 1 - parity) * rows
-        return remote(piece(source, start, rows), sent_mate_sem.at[which, index], mate_sem.at[which, index], mate)
-
-    def from_mate(offset, which):
-        index = (offset + length) % length
-        start = (parity if which == 0 else 1 - parity) * rows
-        ref = weight_buf.at[along(offset) * 2 + 1 - core, pl.ds(pl.multiple_of(start, quarter), rows)]
-        return remote(ref, sent_mate_sem.at[which, index], mate_sem.at[which, index], mate)
-
-    def offsets(step):
-        return [half_way] if step == half_way else [-step, step]
-
-    def serve_ring(step):
+    def turn(way):
+        return 1 if way == 0 else -1
+
+    def part_of(n, way):
+        half = lax.rem(n, 2)
+        return half if way == 0 else 1 - half
+
+    def ring(n, way, hops):
+        source = along(-turn(way) * hops)
+        ref = quarters(source, core, parity * rows + part_of(n, way) * quarter)
+        return remote(ref, sent_ring_sem.at[way, n], ring_sem.at[way, n], at_rank(along(turn(way))))
+
+    def ring_out(n, way):
+        return ring(n, way, n // 2)
+
+    def ring_in(n, way):
+        return ring(n, way, n // 2 + 1)
+
+    def cross(n, way, own_side):
+        part = part_of(n, way)
+        side = parity if own_side else 1 - parity
+        ref = quarters(along(-turn(way) * (n // 2 + 1)), core, side * rows + part * quarter)
+        return remote(ref, sent_cross_sem.at[way, n], cross_sem.at[way, n], across(1 - 2 * part))
+
+    def to_mate(n, way, own_side, kind):
+        side = parity if own_side else 1 - parity
+        ref = quarters(along(-turn(way) * (n // 2 + 1)), kind, side * rows + part_of(n, way) * quarter)
+        which = 0 if own_side else 1
+        return remote(ref, sent_mate_sem.at[way, which, n], mate_sem.at[way, which, n], mate)
+
+    def whole_to_mate(kind):
+        return remote(weight_buf.at[line * 2 + kind], sent_whole_sem, whole_sem, mate)
+
+    def serve_ring(n):
         for way in range(2):
-            ring_arrival(step, way).wait_recv()
-            if step < half_way:
-                ring(step + 1, way).start()
-        for offset in offsets(step):
-            for way in range(2):
-                cross(offset, way).start()
-            to_mate(offset, 0).start()
-
-    served = set()
-
-    def serve_cross(step):
-        served.add(step)
-        for offset in offsets(step):
-            for way in range(2):
-                cross_arrival(offset, way).wait_recv()
-            to_mate(offset, 1).start()
-
-    @pl.loop(0, pairs // batch)
+            ring_in(n, way).wait_recv()
+
+            @pl.when(n + 2 <= last)
+            def _():
+                ring_out(n + 2, way).start()
+
+        for way in range(2):
+            cross(n, way, True).start()
+            to_mate(n, way, True, core).start()
+
+    def serve_cross(n):
+        for way in range(2):
+            cross(n, way, False).wait_recv()
+            to_mate(n, way, False, core).start()
+
+    pl.semaphore_wait(barrier, devices - 1 + 3)
+    own.wait()
+    for n in range(2 if half_way > 1 else 1):
+        for way in range(2):
+            ring_out(n, way).start()
+    whole_to_mate(core).start()
+
+    rounds = pairs // batch
+
+    def serve(n):
+        @pl.when(n <= last)
+        def _():
+            serve_ring(n)
+
+            @pl.when(n >= 2)
+            def _():
+                serve_cross(n - 2)
+
+    for load in loads:
+        load.wait()
+    squashed = jnp.tanh(low_ref[...].astype(F32)).astype(BF16)
+    rate_low = rate_ref[...]
+
+    @pl.loop(0, rounds)
     def _(b):
-        prepare_quads([b * (batch // 2) + i for i in range(batch // 2)])
-
-        @pl.when(b == 0)
-        def _():
-            pl.semaphore_wait(barrier, devices - 1 + 3)
-            own.wait()
-            for way in range(2):
-                ring(1, way).start()
-            for which in range(2):
-                to_mate(0, which).start()
+        wavefront([prepare(size, pl.ds(pl.multiple_of((b * (batch // 2) + i) * QUAD, QUAD), QUAD), q_ref, k_ref,
+                           squashed, rate_low, dup_ref, rup_ref, base_ref, ops, decay_buf,
+                           2 * (b * (batch // 2) + i)) for i in range(batch // 2)])
 
     def head_copy(head, sender, target):
         return pltpu.make_async_remote_copy(
@@ -386,7 +389,7 @@
     @pl.loop(0, pairs // batch)
     def _(b):
         ats = [pl.ds(pl.multiple_of((b * batch + i) * PAIR, PAIR), PAIR) for i in range(batch)]
-        messages = transitions(size, ats, v_ref, ops, solved_bufs)
+        messages = transitions(size, ats, v_ref, ops, solved_bufs, lambda: serve(2 * b))
         for i, (first, second) in enumerate(messages):
             message_buf[2 * (b * batch + i)] = first
             message_buf[2 * (b * batch + i) + 1] = second
@@ -401,25 +404,15 @@
                 head_copy(head, me, {"sp": keeper(head)}).start()
                 decay_copy(head, me, {"sp": keeper(head)}).start()
 
-        @pl.when(b == 0)
-        def _():
-            serve_ring(1)
+        serve(2 * b + 1)
 
     arrive_buf[me] = message_buf[my_head]
     arrive_decay[me] = decay_buf[my_head]
-    serve_cross(1)
-    if half_way > 1:
-        serve_ring(2)
-
     @pl.loop(0, pairs // batch)
     def _(b):
         wavefront([readouts(size, pl.ds(pl.multiple_of((b * batch + i) * PAIR, PAIR), PAIR), v_ref, ops,
                             solved_bufs, local_bufs) for i in range(batch)])
-
-    if half_way > 1:
-        serve_cross(2)
-    if half_way > 2:
-        serve_ring(3)
+        serve(2 * rounds + b)
 
     others = pl.ds(0, devices - 1)
     pltpu.make_async_copy(arrive_buf.at[others], arrive_buf.at[others], message_sem).wait()
@@ -482,9 +475,13 @@
 
     start_buf[my_head] = back_buf[me]
 
-    for step in range(3, half_way):
-        serve_cross(step)
-        serve_ring(step + 1)
+    seen = min(3 * rounds, last + 1)
+    for n in range(seen, last + 1):
+        serve_ring(n)
+    crossed = max(seen - 2, 0)
+    for n in range(crossed, last - 1):
+        serve_cross(n)
+    crossed = max(crossed, last - 1)
 
     mean_ones = cat([same_head_ones(PAIR, 1.0 / HEAD)] * 2, 0)
     centring = jnp.where(lane == row + HEAD, F32(1.0 - 1.0 / HEAD), F32(-1.0 / HEAD)).astype(BF16)
@@ -522,32 +519,29 @@
         weight = cat([weight_buf[2 * at], weight_buf[2 * at + 1]], 1)
         out_ref[:, pl.ds(pl.multiple_of(at * QUAD, QUAD), QUAD)] = mm(mix_buf[...], weight).astype(BF16)
 
-    last = [step for step in range(1, half_way + 1) if step not in served]
-    early = [offset for step in range(1, half_way) for offset in offsets(step)]
-    for offset in [0] + early:
-        for which in range(2):
-            from_mate(offset, which).wait_recv()
-    for step in last:
-        serve_cross(step)
-    for offset in [0] + early:
+    for n in range(crossed, last + 1):
+        serve_cross(n)
+    whole_to_mate(1 - core).wait_recv()
+    project(0)
+    for n in range(last + 1):
+        for way in range(2):
+            for own_side in (True, False):
+                to_mate(n, way, own_side, 1 - core).wait_recv()
+    for offset in [o for step in range(1, half_way) for o in (-step, step)] + [half_way]:
         project(offset)
-    for which in range(2):
-        from_mate(half_way, which).wait_recv()
-    project(half_way)
 
     pltpu.make_async_copy(message_buf.at[others], message_buf.at[others], sent_sem).wait()
     pltpu.make_async_copy(decay_buf.at[others], decay_buf.at[others], sent_decay_sem).wait()
     pltpu.make_async_copy(back_buf.at[others], back_buf.at[others], sent_back_sem).wait()
-    for step in range(1, half_way + 1):
+    whole_to_mate(core).wait_send()
+
+    @pl.loop(0, last + 1)
+    def _(n):
         for way in range(2):
-            ring(step, way).wait_send()
-        for offset in offsets(step):
-            for way in range(2):
-                cross(offset, way).wait_send()
-            for which in range(2):
-                to_mate(offset, which).wait_send()
-    for which in range(2):
-        to_mate(0, which).wait_send()
+            ring_out(n, way).wait_send()
+            for own_side in (True, False):
+                to_mate(n, way, own_side, core).wait_send()
+            cross(n, way, True).wait_send()
 
 
 def per_device(devices, ranks, query_rows, key_rows, value_rows, decay_low, rate_low, decay_up, rate_up,
@@ -556,16 +550,18 @@
     heads = width // HEAD
     batch = min(8, width // PAIR)
     length = ranks // 2
-    half_way = length // 2
+    pieces = 2 * (length // 2) - 1
+    anywhere = pl.BlockSpec(memory_space=pl.ANY)
     vmem = pl.BlockSpec(memory_space=pltpu.VMEM)
     dma = pltpu.SemaphoreType.DMA
     wide = lambda lanes: pltpu.VMEM((size, lanes), BF16)
     out = pl.pallas_call(
         functools.partial(mixer_kernel, devices, ranks, batch),
-        in_specs=[vmem] * 9 + [pl.BlockSpec(memory_space=pl.ANY)],
+        in_specs=[anywhere] * 3 + [vmem] * 2 + [anywhere] * 2 + [vmem] * 2 + [anywhere],
         out_specs=vmem,
         out_shape=jax.ShapeDtypeStruct((size, out_weight.shape[1] * ranks), BF16),
-        scratch_shapes=[wide(width) for _ in range(10)] + [pltpu.VMEM((size, width), F32)] * 2
+        scratch_shapes=[wide(width)] * 3 + [pltpu.VMEM(decay_up.shape, BF16)] * 2 + [dma((5,))]
+        + [wide(width) for _ in range(10)] + [pltpu.VMEM((size, width), F32)] * 2
         + [wide(2 * width) for _ in range(4)] + [wide(width)] + [
             pltpu.VMEM((heads, HEAD, PAIR), BF16),
             pltpu.VMEM((heads, 1, PAIR), F32),
@@ -575,8 +571,8 @@
             pltpu.VMEM((heads, HEAD // 2, PAIR), BF16),
             pltpu.VMEM((ranks,) + out_weight.shape, BF16),
             dma, dma, dma((heads,)), dma, dma, dma,
-            dma((half_way,)), dma((half_way,)), dma((2, length)), dma((2, length)),
-            dma((2, half_way)), dma((2, length)), dma((2, length)), dma,
+            dma((2, pieces)), dma((2, pieces)), dma((2, 2, pieces)), dma,
+            dma((2, pieces)), dma((2, pieces)), dma((2, 2, pieces)), dma, dma,
         ],
         compiler_params=pltpu.CompilerParams(
             collective_id=0, has_side_effects=True, vmem_limit_bytes=60 * 2**20),

time: 64.8 us -> 63.5 us (0.980)
  Pallas kernels: 62.3 us -> 61.3 us
    pallas_call x1, Pallas kernels: 62.3 us -> 61.3 us  [per_device(): pl.pallas_call(functools.partial(mixer_kernel, devices, ranks, batch), in...]
where the time goes in v5:
time: 63.5 us; the launch traced here: 63.2 us
  Pallas kernels  61.3 us (97%)
  local copies, waits for them, and re-layouts  1.88 us (3%)
    pallas_call x1, Pallas kernels, per_device(): pl.pallas_call(functools.partial(mixer_kernel, devices, ranks, batch), in...  61.3 us
    unnamed x1, local copies, waits for them, and re-layouts  1.88 us

profile of v5, /device:TPU:1, one launch (start us, length us, event | category | flops | bytes accessed | tf_op | source)
XLA Modules:
  0.0 63.2 jit_solution(9415305879244657421)
XLA Ops:
  0.0 61.3 %mixer.1 = bf16[128,2048]{1,0:T(8,128)(2,1)} custom-call(bf16[128,2048]{1,0:T(8,128)(2,1)} %bitcast.9, bf16[128,2048]{1,0:T(8,128)(2,1)} %bitcast.10, bf16[128,2048]{1,0:T(8,128)(2,1)} %bitcast.11, bf16[128,128]{1,0:T(8,128)(2,1)} %bitcast.12, bf16[128,128]{1,0:T(8,128)(2,1)} %bitcast.13, bf16[128,2048]{1,0:T(8,128)(2,1)} %dup_in.1, ...), custom_call_target="tpu_custom_call" | custom-call | flops 10000000000 | bytes 10000000 | tf_op jit(solution)/shard_map/mixer/pallas_call | solution.py:558
  61.4 1.9 %copy.12 = bf16[1,128,2048]{2,1,0:T(8,128)(2,1)} copy(bf16[1,128,2048]{2,1,0:T(8,128)(2,1)} %bitcast.8) | data formatting | bytes 1048576

commit v6 on v5

--- a/solution.py
+++ b/solution.py
@@ -414,6 +414,9 @@
                             solved_bufs, local_bufs) for i in range(batch)])
         serve(2 * rounds + b)
 
+    seen = min(3 * rounds, last + 1)
+    for n in range(seen, last + 1):
+        serve_ring(n)
     others = pl.ds(0, devices - 1)
     pltpu.make_async_copy(arrive_buf.at[others], arrive_buf.at[others], message_sem).wait()
     pltpu.make_async_copy(arrive_decay.at[others], arrive_decay.at[others], decay_sem).wait()
@@ -475,13 +478,8 @@
 
     start_buf[my_head] = back_buf[me]
 
-    seen = min(3 * rounds, last + 1)
-    for n in range(seen, last + 1):
-        serve_ring(n)
-    crossed = max(seen - 2, 0)
-    for n in range(crossed, last - 1):
+    for n in range(max(seen - 2, 0), last + 1):
         serve_cross(n)
-    crossed = max(crossed, last - 1)
 
     mean_ones = cat([same_head_ones(PAIR, 1.0 / HEAD)] * 2, 0)
     centring = jnp.where(lane == row + HEAD, F32(1.0 - 1.0 / HEAD), F32(-1.0 / HEAD)).astype(BF16)
@@ -519,8 +517,6 @@
         weight = cat([weight_buf[2 * at], weight_buf[2 * at + 1]], 1)
         out_ref[:, pl.ds(pl.multiple_of(at * QUAD, QUAD), QUAD)] = mm(mix_buf[...], weight).astype(BF16)
 
-    for n in range(crossed, last + 1):
-        serve_cross(n)
     whole_to_mate(1 - core).wait_recv()
     project(0)
     for n in range(last + 1):

time: 63.5 us -> 61.8 us (0.973)
  the two profiles are of different devices: /device:TPU:1 before, /device:TPU:30 now
where the time goes in v6:
time: 61.8 us; the launch traced here: 61.6 us
  Pallas kernels  59.7 us (97%)
  local copies, waits for them, and re-layouts  1.88 us (3%)
    pallas_call x1, Pallas kernels, per_device(): pl.pallas_call(functools.partial(mixer_kernel, devices, ranks, batch), in...  59.7 us
    unnamed x1, local copies, waits for them, and re-layouts  1.88 us

profile of v6, /device:TPU:30, one launch (start us, length us, event | category | flops | bytes accessed | tf_op | source)
XLA Modules:
  0.0 61.6 jit_solution(2866611713146546454)
XLA Ops:
  0.0 59.7 %mixer.1 = bf16[128,2048]{1,0:T(8,128)(2,1)} custom-call(bf16[128,2048]{1,0:T(8,128)(2,1)} %bitcast.9, bf16[128,2048]{1,0:T(8,128)(2,1)} %bitcast.10, bf16[128,2048]{1,0:T(8,128)(2,1)} %bitcast.11, bf16[128,128]{1,0:T(8,128)(2,1)} %bitcast.12, bf16[128,128]{1,0:T(8,128)(2,1)} %bitcast.13, bf16[128,2048]{1,0:T(8,128)(2,1)} %dup_in.1, ...), custom_call_target="tpu_custom_call" | custom-call | flops 10000000000 | bytes 10000000 | tf_op jit(solution)/shard_map/mixer/pallas_call | solution.py:554
  59.7 1.9 %copy.12 = bf16[1,128,2048]{2,1,0:T(8,128)(2,1)} copy(bf16[1,128,2048]{2,1,0:T(8,128)(2,1)} %bitcast.8) | data formatting | bytes 1048576
